TPU v7x, 32 devices: a whole 2x2x4 slice. The times are simulated.
32 devices in a mesh: tp: 8 (over z, core), dp: 4 (over y, x).
Axes of the slice: x: 2, y: 2, z: 4, core: 2. Of those that a mesh axis runs over, the one named last changes fastest.
Arguments:
- tokens: bfloat16 [32, 4096], P('tp', 'dp'), may hold values from -6 to 6
- norm_gain: bfloat16 [2, 4096], P(None, 'dp'), may hold values from 0.099609375 to 1.8984375
- w_query: bfloat16 [2, 4096, 1024], P(None, 'dp', 'tp'), may hold values from -0.09375 to 0.09375
- w_key: bfloat16 [2, 4096, 1024], P(None, 'dp', 'tp'), may hold values from -0.09375 to 0.09375
- w_value: bfloat16 [2, 4096, 1024], P(None, 'dp', 'tp'), may hold values from -0.09375 to 0.09375
- w_outgate: bfloat16 [2, 4096, 1024], P(None, 'dp', 'tp'), may hold values from -0.09375 to 0.09375
- w_gates: bfloat16 [2, 4096, 16], P(None, 'dp'), may hold values from -0.09375 to 0.09375
- gate_bias: float32 [2, 2, 8], P(None, None, 'tp'), may hold values from -1 to 5
- w_out: bfloat16 [2, 1024, 4096], P(None, 'tp', 'dp'), may hold values from -0.1875 to 0.1875
- memory: float32 [2, 32, 8, 128, 128], P(None, 'dp', 'tp'), may hold values from -6 to 6
- normalizer: float32 [2, 32, 8, 128], P(None, 'dp', 'tp'), may hold values from -3 to 3
- stabilizer: float32 [2, 32, 8], P(None, 'dp', 'tp'), may hold values from -8 to 300, as said below
Outputs:
- mixed: bfloat16 [32, 4096], P('tp', 'dp')
- new_memory: float32 [2, 32, 8, 128, 128], P(None, 'dp', 'tp')
- new_normalizer: float32 [2, 32, 8, 128], P(None, 'dp', 'tp')
- new_stabilizer: float32 [2, 32, 8], P(None, 'dp', 'tp')
Inputs may be any that keep to these rules, and one draw needn't show every extreme that they name: `stabilizer`: lies between -8 and 8, except that some entries may be as large as 300.
All inputs are finite; a program needn't handle non-finite values.
Results may differ from a plain program's by a relative error of at most 0.04.
Values may be sent and summed in bfloat16 or wider, within the bound.
A program may use at most 64 MiB of HBM per device.

v0:
```python
import jax
import jax.numpy as jnp
from jax import lax
from jax.sharding import PartitionSpec as P

D = 4096
HEAD_SIZE = 128


epsilon = 1e-06


def cell_update(query, key_rows, value_rows, input_pre, forget_pre, memory, normalizer, stabilizer):
    batch_size = query.shape[0]
    head_count = input_pre.shape[1]
    query_float = query.astype(jnp.float32).reshape(batch_size, head_count, -1)
    key_float = key_rows.astype(jnp.float32).reshape(
        batch_size, head_count, -1
    ) * query_float.shape[2] ** (-0.5)
    value_float = value_rows.astype(jnp.float32).reshape(batch_size, head_count, -1)
    carried = jax.nn.log_sigmoid(forget_pre) + stabilizer
    new_max = jnp.maximum(carried, input_pre)
    keep_factor = jnp.exp(carried - new_max)
    write_factor = jnp.exp(input_pre - new_max)
    new_memory = (
        keep_factor[:, :, None, None] * memory
        + write_factor[:, :, None, None] * value_float[:, :, :, None] * key_float[:, :, None, :]
    )
    new_normalizer = keep_factor[:, :, None] * normalizer + write_factor[:, :, None] * key_float
    numerator = jnp.sum(new_memory * query_float[:, :, None, :], axis=3)
    denominator = jnp.sum(new_normalizer * query_float, axis=2)
    floor_value = jnp.maximum(jnp.abs(denominator), jnp.exp(-new_max))
    readout = numerator / jnp.maximum(floor_value, 1.0)[:, :, None]
    return (readout.reshape(batch_size, -1), new_memory, new_normalizer, new_max)


def finish_split(partial_out, wide_rows):
    summed = lax.psum_scatter(partial_out, "tp", scatter_dimension=0, tiled=True)
    own_rows = lax.dynamic_slice_in_dim(
        wide_rows, lax.axis_index("tp") * summed.shape[0], summed.shape[0], 0
    )
    return (own_rows + summed).astype(jnp.bfloat16)


def body(
    tokens,
    norm_gain,
    w_query,
    w_key,
    w_value,
    w_outgate,
    w_gates,
    gate_bias,
    w_out,
    memory,
    normalizer,
    stabilizer,
):
    heads_here = w_query.shape[2] // HEAD_SIZE
    seq_here = memory.shape[1]
    all_heads = w_gates.shape[2] // 2
    head_first = lax.axis_index("tp") * heads_here
    seq_first = lax.axis_index("dp") * seq_here
    current = tokens
    gathered = None
    memories = []
    normalizers = []
    maxima = []
    for layer_index in range(2):
        if gathered is None:
            gathered = lax.all_gather(current, "tp", axis=0, tiled=True)
        wide_rows = gathered.astype(jnp.float32)
        square_part = jnp.sum(wide_rows * wide_rows, axis=1)
        scaled = (wide_rows * norm_gain[layer_index].astype(jnp.float32)[None, :]).astype(
            jnp.bfloat16
        )
        gate_weight = w_gates[layer_index]
        own_gates = jnp.concatenate(
            [
                lax.dynamic_slice_in_dim(gate_weight, head_first, heads_here, 1),
                lax.dynamic_slice_in_dim(gate_weight, all_heads + head_first, heads_here, 1),
            ],
            axis=1,
        )
        term_query = jnp.dot(scaled, w_query[layer_index], preferred_element_type=jnp.float32)
        term_key = jnp.dot(scaled, w_key[layer_index], preferred_element_type=jnp.float32)
        term_value = jnp.dot(scaled, w_value[layer_index], preferred_element_type=jnp.float32)
        term_outgate = jnp.dot(scaled, w_outgate[layer_index], preferred_element_type=jnp.float32)
        term_gates = jnp.dot(scaled, own_gates, preferred_element_type=jnp.float32)
        square_all = lax.psum(square_part, "dp")
        square_own = lax.dynamic_slice_in_dim(square_all, seq_first, seq_here, 0)
        sum_query, sum_key, sum_value, sum_outgate, sum_gates = (
            lax.psum_scatter(term_query, "dp", scatter_dimension=0, tiled=True),
            lax.psum_scatter(term_key, "dp", scatter_dimension=0, tiled=True),
            lax.psum_scatter(term_value, "dp", scatter_dimension=0, tiled=True),
            lax.psum_scatter(term_outgate, "dp", scatter_dimension=0, tiled=True),
            lax.psum_scatter(term_gates, "dp", scatter_dimension=0, tiled=True),
        )
        inv_scale = lax.rsqrt(square_own / D + epsilon)[:, None]
        query = (sum_query * inv_scale).astype(jnp.bfloat16)
        key_rows = (sum_key * inv_scale).astype(jnp.bfloat16)
        value_rows = (sum_value * inv_scale).astype(jnp.bfloat16)
        outgate = (sum_outgate * inv_scale).astype(jnp.bfloat16)
        gate_pre = sum_gates * inv_scale
        bias_here = gate_bias[layer_index]
        input_pre = gate_pre[:, :heads_here] + bias_here[0][None, :]
        forget_pre = gate_pre[:, heads_here:] + bias_here[1][None, :]
        readout, new_memory, new_normalizer, new_max = cell_update(
            query,
            key_rows,
            value_rows,
            input_pre,
            forget_pre,
            memory[layer_index],
            normalizer[layer_index],
            stabilizer[layer_index],
        )
        gated = (jax.nn.sigmoid(outgate.astype(jnp.float32)) * readout).astype(jnp.bfloat16)
        out_weight = w_out[layer_index]
        partial_out = jnp.dot(
            lax.all_gather(gated, "dp", axis=0, tiled=True),
            out_weight,
            preferred_element_type=jnp.float32,
        )
        if layer_index == 0:
            summed = lax.psum(partial_out, "tp")
            gathered = (wide_rows + summed).astype(jnp.bfloat16)
        else:
            current = finish_split(partial_out, wide_rows)
        memories.append(new_memory)
        normalizers.append(new_normalizer)
        maxima.append(new_max)
    return (current, jnp.stack(memories), jnp.stack(normalizers), jnp.stack(maxima))


def solution(mesh):
    placed = (
        P("tp", "dp"),
        P(None, "dp"),
        P(None, "dp", "tp"),
        P(None, "dp", "tp"),
        P(None, "dp", "tp"),
        P(None, "dp", "tp"),
        P(None, "dp", None),
        P(None, None, "tp"),
        P(None, "tp", "dp"),
        P(None, "dp", "tp", None, None),
        P(None, "dp", "tp", None),
        P(None, "dp", "tp"),
    )
    return jax.shard_map(
        body,
        mesh=mesh,
        in_specs=placed,
        out_specs=(
            P("tp", "dp"),
            P(None, "dp", "tp", None, None),
            P(None, "dp", "tp", None),
            P(None, "dp", "tp"),
        ),
        check_vma=False,
    )
```

profile of v0, /device:TPU:0, one launch (start us, length us, event | category | flops | bytes accessed | tf_op | source)
XLA Modules:
  0.0 269.4 jit_solution(6725401215718095154)
XLA Ops:
  7.2 0.8 slice_convert_fusion
  8.0 15.9 %all-gather = bf16[8,4,1024]{2,1,0:T(4,128)(2,1)S(1)} all-gather(bf16[1,4,1024]{2,1,0:T(4,128)(2,1)} %bitcast.146), channel_id=1, replica_groups=mesh['tp'=8,'dp'=4] {'tp'}, dimensions={0}, use_global_device_ids=true | all-gather | bytes 73728 | tf_op jit(solution)/shard_map/all_gather | solution.py:71
  24.6 1.7 fusion.18
  26.3 0.8 fusion.20
  27.1 0.8 fusion.22
  27.9 1.8 fusion.24
  29.7 0.7 fusion.42
  32.4 40.8 %all-reduce.24.cloned.1.call-done = (f32[32,128]{1,0:T(8,128)}, f32[32]{0:T(128)}, f32[32,128]{1,0:T(8,128)}, f32[32,128]{1,0:T(8,128)}, f32[32,2]{0,1:T(2,128)}, /*index=5*/f32[32,128]{1,0:T(8,128)}) async-done(((f32[32,128]{1,0:T(8,128)}, f32[32]{0:T(128)}, f32[32,128]{1,0:T(8,128)}, f32[32,128]{1,0:T(8,128)}, f32[32,2]{0,1:T(2,128)}, /*index=5*/f32[32,128]{1,0:T(8,128)}), (f32[32,128]{1,0:T(8,128)}, ...) | async-done | bytes 65936
  73.2 0.7 add_rsqrt_fusion.1
  74.0 0.7 fusion.62
  74.7 1.4 broadcast_multiply_fusion.1
  76.1 0.8 fusion.59
  76.8 0.9 multiply_reduce_fusion.3
  78.1 0.8 multiply_convert_fusion.3
  78.9 8.9 %all_gather.10 = bf16[32,128]{1,0:T(8,128)(2,1)S(1)} all-gather(bf16[8,128]{1,0:T(8,128)(2,1)S(1)} %multiply_convert_fusion.3), channel_id=1, replica_groups=mesh['tp'=8,'dp'=4] {'dp'}, dimensions={0}, use_global_device_ids=true | all-gather | bytes 10240 | tf_op jit(solution)/shard_map/all_gather | solution.py:121
  87.8 0.8 fusion.16
  88.7 55.4 %all-reduce.18.cloned.1.call-done = f32[32,1024]{1,0:T(8,128)} async-done(((f32[32,1024]{1,0:T(8,128)}), f32[32,1024]{1,0:T(8,128)}) %all-reduce.18.cloned.1.call-update) | async-done | bytes 131088 | tf_op jit(solution)/shard_map/psum | solution.py:126
  144.1 1.5 multiply_reduce_fusion
  145.7 0.8 fusion.8
  146.5 0.8 fusion.10
  147.2 0.8 fusion.12
  148.0 0.8 fusion.14
  151.4 38.9 %all-reduce.22.cloned.1.call-done = (f32[32,128]{1,0:T(8,128)}, f32[32]{0:T(128)}, f32[32,128]{1,0:T(8,128)}, f32[32,128]{1,0:T(8,128)}, f32[32,2]{0,1:T(2,128)}, /*index=5*/f32[32,128]{1,0:T(8,128)}) async-done(((f32[32,128]{1,0:T(8,128)}, f32[32]{0:T(128)}, f32[32,128]{1,0:T(8,128)}, f32[32,128]{1,0:T(8,128)}, f32[32,2]{0,1:T(2,128)}, /*index=5*/f32[32,128]{1,0:T(8,128)}), (f32[32,128]{1,0:T(8,128)}, ...) | async-done | bytes 65936
  191.8 1.3 broadcast_multiply_fusion
  193.1 0.8 fusion.58
  193.9 0.9 multiply_reduce_fusion.2
  195.6 0.8 multiply_convert_fusion.2
  196.3 8.9 %all_gather.11 = bf16[32,128]{1,0:T(8,128)(2,1)S(1)} all-gather(bf16[8,128]{1,0:T(8,128)(2,1)S(1)} %multiply_convert_fusion.2), channel_id=1, replica_groups=mesh['tp'=8,'dp'=4] {'dp'}, dimensions={0}, use_global_device_ids=true | all-gather | bytes 10240 | tf_op jit(solution)/shard_map/all_gather | solution.py:121
  205.2 0.8 fusion.6
  206.7 1.1 pad_maximum_fusion
  208.3 53.2 %all-reduce.20.cloned.1.call-done = f32[32,1024]{1,0:T(8,128)} async-done(((f32[32,1024]{1,0:T(8,128)}), f32[32,1024]{1,0:T(8,128)}) %all-reduce.20.cloned.1.call-update) | async-done | bytes 131088
  261.5 1.4 fusion.37
  (57 shorter events, 8.0 us)
Async XLA Ops:
  7.2 19.1 %copy-start.2 = (bf16[2,1024,128]{2,1,0:T(8,128)(2,1)S(1)}, bf16[2,1024,128]{2,1,0:T(8,128)(2,1)}, u32[]{:S(2)}) copy-start(bf16[2,1024,128]{2,1,0:T(8,128)(2,1)} %param.15) | copy-start | bytes 1572868
  7.2 66.0 %all-reduce.24.cloned.1.call-start = ((), (), s32[]{:S(2)}) async-start(), calls=%async_computation.3 | async-start | bytes 134144
  23.9 3.2 %copy-start.3 = (bf16[2,1024,128]{2,1,0:T(8,128)(2,1)S(1)}, bf16[2,1024,128]{2,1,0:T(8,128)(2,1)}, u32[]{:S(2)}) copy-start(bf16[2,1024,128]{2,1,0:T(8,128)(2,1)} %param.16) | copy-start | bytes 1572868
  23.9 5.7 %copy-start.6 = (bf16[2,1024,16]{1,2,0:T(8,128)(2,1)S(1)}, bf16[2,1024,16]{1,2,0:T(8,128)(2,1)}, u32[]{:S(2)}) copy-start(bf16[2,1024,16]{1,2,0:T(8,128)(2,1)} %param.18) | copy-start | bytes 196612
  23.9 53.8 %copy-start = (f32[2,8,1,128,128]{4,3,2,1,0:T(8,128)S(1)}, f32[2,8,1,128,128]{4,3,2,1,0:T(8,128)}, u32[]{:S(2)}) copy-start(f32[2,8,1,128,128]{4,3,2,1,0:T(8,128)} %param.21) | copy-start | bytes 3145732
  27.8 2.6 copy-start.13
  27.9 3.9 %copy-start.8 = (f32[2,2,1]{1,2,0:T(1,128)S(1)}, f32[2,2,1]{1,2,0:T(1,128)}, u32[]{:S(2)}) copy-start(f32[2,2,1]{1,2,0:T(1,128)} %param.19) | copy-start | bytes 52
  27.9 46.8 %copy-start.9 = (f32[2,8,1]{1,2,0:T(1,128)S(1)}, f32[2,8,1]{1,2,0:T(1,128)}, u32[]{:S(2)}) copy-start(f32[2,8,1]{1,2,0:T(1,128)} %param.23) | copy-start | bytes 196
  27.9 48.2 %copy-start.7 = (f32[2,8,1,128]{3,2,1,0:T(1,128)S(1)}, f32[2,8,1,128]{3,2,1,0:T(1,128)}, u32[]{:S(2)}) copy-start(f32[2,8,1,128]{3,2,1,0:T(1,128)} %param.22) | copy-start | bytes 24580
  29.6 58.1 %copy-start.5 = (bf16[2,128,1024]{2,1,0:T(8,128)(2,1)S(1)}, bf16[2,128,1024]{2,1,0:T(8,128)(2,1)}, u32[]{:S(2)}) copy-start(bf16[2,128,1024]{2,1,0:T(8,128)(2,1)} %param.20) | copy-start | bytes 1572868
  30.4 113.7 %all-reduce.18.cloned.1.call-start = ((), (), s32[]{:S(2)}) async-start(), calls=%async_computation | async-start | bytes 262144 | tf_op jit(solution)/shard_map/psum | solution.py:126
  87.8 57.9 %copy-start.1 = (bf16[2,1024,128]{2,1,0:T(8,128)(2,1)S(1)}, bf16[2,1024,128]{2,1,0:T(8,128)(2,1)}, u32[]{:S(2)}) copy-start(bf16[2,1024,128]{2,1,0:T(8,128)(2,1)} %param.14) | copy-start | bytes 1572868
  88.6 101.7 %all-reduce.22.cloned.1.call-start = ((), (), s32[]{:S(2)}) async-start(), calls=%async_computation.2 | async-start | bytes 134144
  145.7 2.3 copy-start.4
  149.5 112.0 %all-reduce.20.cloned.1.call-start = ((), (), s32[]{:S(2)}) async-start(), calls=%async_computation.1 | async-start | bytes 262144
  149.5 0.7 copy-start.12
  190.4 0.7 copy-start.11
  191.1 0.6 copy-start.10
Sparse Core Ops, SparseCore 0:
  30.5 42.6 all-reduce.23
  88.8 55.2 all-reduce.17
  149.6 40.6 all-reduce.21
  206.2 55.2 all-reduce.19
where the time goes:
time: 270 us; the launch traced here: 269 us
  waiting for transfers between devices  188 us (70%)
  blocking collectives  33.7 us (12%)
  other arithmetic  16.8 us (6%)
  between operations  15.2 us (6%)
  matrix products  11.1 us (4%)
  local copies, waits for them, and re-layouts  3.91 us (1%)
    unnamed x7, waiting for transfers between devices  133 us
    psum x1, waiting for transfers between devices, body(): summed = lax.psum(partial_out, 'tp')  55.4 us
    all_gather x2, blocking collectives, body(): lax.all_gather(gated, 'dp', axis=0, tiled=True)  17.8 us
    all_gather x1, blocking collectives, body(): gathered = lax.all_gather(current, 'tp', axis=0, tiled=True)  15.9 us
  transfers between devices with their start and end apart: 4, of which 4 were waited for; matrix products, arithmetic and copies ran while one was open for 2% of the time, Pallas kernels for 0%

commit v1 on v0

v1 whole, which is shorter than its diff:
```python
import functools

import jax
import jax.numpy as jnp
from jax import lax
from jax.experimental import pallas as pl
from jax.experimental.pallas import tpu as pltpu
from jax.sharding import PartitionSpec as P

HEAD_SIZE = 128
MESH = pl.DeviceIdType.MESH
EPSILON = 1e-06
F32 = jnp.float32
BF16 = jnp.bfloat16


def kernel(
    n_tp,
    n_dp,
    tokens,
    norm_gain,
    w_query,
    w_key,
    w_value,
    w_outgate,
    w_gates,
    gate_bias,
    w_out,
    memory,
    normalizer,
    stabilizer,
    mixed,
    new_memory,
    new_normalizer,
    new_stabilizer,
    gain_v,
    w_in_v,
    w_gates_v,
    bias_v,
    w_out_v,
    mem_v,
    norm_v,
    stab_v,
    new_mem_v,
    own_x,
    x_slots,
    send_q,
    recv_q,
    send_g,
    recv_g,
    own_gated,
    gated_slots,
    send_o,
    recv_o,
    in_sem,
    w_sem,
    mem_sem,
    out_sem,
    ag_send,
    ag_recv,
    rq_send,
    rq_recv,
    rg_send,
    rg_recv,
    gd_send,
    gd_recv,
    ro_send,
    ro_recv,
):
    tp = lax.axis_index("tp")
    dp = lax.axis_index("dp")
    seqs = mem_v.shape[1]
    rows = own_x.shape[1]
    width = own_x.shape[2]
    total = n_tp * rows
    heads = w_gates_v.shape[1] // 2
    features = width * n_dp

    def tp_peer(off):
        return lax.rem(tp + off, n_tp)

    def dp_peer(off):
        return lax.rem(dp + off, n_dp)

    barrier = pltpu.get_barrier_semaphore()
    tok_copy = pltpu.make_async_copy(tokens, own_x.at[0], in_sem.at[0])
    tok_copy.start()
    for off in range(1, n_tp):
        pl.semaphore_signal(barrier, inc=1, device_id={"tp": tp_peer(off)}, device_id_type=MESH)
    for off in range(1, n_dp):
        pl.semaphore_signal(barrier, inc=1, device_id={"dp": dp_peer(off)}, device_id_type=MESH)

    small = [
        pltpu.make_async_copy(norm_gain, gain_v, in_sem.at[1]),
        pltpu.make_async_copy(w_gates, w_gates_v, in_sem.at[2]),
        pltpu.make_async_copy(gate_bias, bias_v, in_sem.at[3]),
        pltpu.make_async_copy(normalizer, norm_v, in_sem.at[4]),
        pltpu.make_async_copy(stabilizer, stab_v, in_sem.at[5]),
    ]
    for copy in small:
        copy.start()
    w_copies, out_copies, mem_copies = [], [], []
    for layer in range(2):
        w_copies.append(
            [
                pltpu.make_async_copy(
                    ref.at[layer],
                    w_in_v.at[layer, :, pl.ds(i * HEAD_SIZE, HEAD_SIZE)],
                    w_sem.at[layer, i],
                )
                for i, ref in enumerate((w_query, w_key, w_value, w_outgate))
            ]
        )
        mem_copies.append(pltpu.make_async_copy(memory.at[layer], mem_v.at[layer], mem_sem.at[layer]))
        out_copies.append(pltpu.make_async_copy(w_out.at[layer], w_out_v.at[layer], w_sem.at[layer, 4]))
        for copy in w_copies[layer]:
            copy.start()
        mem_copies[layer].start()
        out_copies[layer].start()

    tok_copy.wait()
    pl.semaphore_wait(barrier, n_tp + n_dp - 2)

    started = []

    def send_tp(src, dst, send_sem, recv_sem, off):
        copy = pltpu.make_async_remote_copy(
            src_ref=src,
            dst_ref=dst,
            send_sem=send_sem,
            recv_sem=recv_sem,
            device_id={"tp": tp_peer(off)},
            device_id_type=MESH,
        )
        copy.start()
        started.append(copy)
        return copy

    def send_dp(src, dst, send_sem, recv_sem, off):
        copy = pltpu.make_async_remote_copy(
            src_ref=src,
            dst_ref=dst,
            send_sem=send_sem,
            recv_sem=recv_sem,
            device_id={"dp": dp_peer(off)},
            device_id_type=MESH,
        )
        copy.start()
        started.append(copy)
        return copy

    def gather_x(layer):
        copies = [
            send_tp(
                own_x.at[layer],
                x_slots.at[layer, tp],
                ag_send.at[layer, off],
                ag_recv.at[layer, off],
                off,
            )
            for off in range(1, n_tp)
        ]
        x_slots[layer, tp] = own_x[layer]
        return copies

    lane = lax.broadcasted_iota(jnp.int32, (total, HEAD_SIZE), 1)
    diag_seq = lax.broadcasted_iota(jnp.int32, (seqs, seqs), 0) == lax.broadcasted_iota(
        jnp.int32, (seqs, seqs), 1
    )
    sub = lax.broadcasted_iota(jnp.int32, (seqs, HEAD_SIZE), 0)
    scale = HEAD_SIZE ** (-0.5)
    nt = (((1,), (1,)), ((), ()))
    tn = (((0,), (0,)), ((), ()))
    updates = []

    ag = gather_x(0)
    for copy in small:
        copy.wait()
    for layer in range(2):
        for copy in w_copies[layer]:
            copy.wait()
        mem_copies[layer].wait()
        mem = mem_v[layer].reshape(seqs * HEAD_SIZE, HEAD_SIZE)
        mem_hi = mem.astype(BF16)
        mem_lo = (mem - mem_hi.astype(F32)).astype(BF16)
        gain = gain_v[pl.ds(layer, 1), :].astype(F32)

        for copy in ag:
            copy.wait_recv()
        wide = jnp.concatenate([x_slots[layer, t].astype(F32) for t in range(n_tp)], axis=0)
        scaled = (wide * gain).astype(BF16)
        terms = jnp.dot(scaled, w_in_v[layer], preferred_element_type=F32).astype(BF16)
        for d in range(n_dp):
            send_q[layer, d] = terms[d * seqs : (d + 1) * seqs]
        rq = [
            send_dp(
                send_q.at[layer, dp_peer(off)],
                recv_q.at[layer, off],
                rq_send.at[layer, off],
                rq_recv.at[layer, off],
                off,
            )
            for off in range(1, n_dp)
        ]
        squares = jnp.sum(wide * wide, axis=1, keepdims=True)
        gates = lax.dot_general(scaled, w_gates_v[layer], nt, preferred_element_type=F32)
        column = lax.broadcasted_iota(jnp.int32, gates.shape, 1)
        gate_in = jnp.sum(jnp.where(column == tp, gates, 0.0), axis=1, keepdims=True)
        gate_forget = jnp.sum(jnp.where(column == heads + tp, gates, 0.0), axis=1, keepdims=True)
        packed = jnp.where(
            lane == 0, gate_in, jnp.where(lane == 1, gate_forget, jnp.where(lane == 2, squares, 0.0))
        )
        for d in range(n_dp):
            send_g[layer, d] = packed[d * seqs : (d + 1) * seqs]
        rg = [
            send_dp(
                send_g.at[layer, dp_peer(off)],
                recv_g.at[layer, off],
                rg_send.at[layer, off],
                rg_recv.at[layer, off],
                off,
            )
            for off in range(1, n_dp)
        ]

        sums = send_q[layer, dp].astype(F32)
        small_sums = send_g[layer, dp]
        for off in range(1, n_dp):
            rq[off - 1].wait_recv()
            sums = sums + recv_q[layer, off].astype(F32)
        for off in range(1, n_dp):
            rg[off - 1].wait_recv()
            small_sums = small_sums + recv_g[layer, off]
        inv = lax.rsqrt(small_sums[:, 2:3] / features + EPSILON)
        held = (sums * inv).astype(BF16)
        query = held[:, :HEAD_SIZE]
        key = held[:, HEAD_SIZE : 2 * HEAD_SIZE]
        value = held[:, 2 * HEAD_SIZE : 3 * HEAD_SIZE]
        outgate = held[:, 3 * HEAD_SIZE :].astype(F32)
        bias = bias_v[layer]
        pre_in = small_sums[:, 0:1] * inv + bias[:, 0:1]
        pre_forget = small_sums[:, 1:2] * inv + bias[:, 1:2]
        old_max = jnp.sum(
            jnp.where(diag_seq, jnp.broadcast_to(stab_v[layer], (seqs, seqs)), 0.0),
            axis=1,
            keepdims=True,
        )
        carried = jnp.minimum(pre_forget, 0.0) - jnp.log1p(jnp.exp(-jnp.abs(pre_forget))) + old_max
        new_max = jnp.maximum(carried, pre_in)
        keep = jnp.exp(carried - new_max)
        write = jnp.exp(pre_in - new_max)
        query_f = query.astype(F32)
        key_f = key.astype(F32) * scale
        value_f = value.astype(F32)
        new_norm = keep * norm_v[layer].reshape(seqs, HEAD_SIZE) + write * key_f
        denominator = jnp.sum(new_norm * query_f, axis=1, keepdims=True)
        key_query = jnp.sum(key_f * query_f, axis=1, keepdims=True)
        read = lax.dot_general(query, mem_hi, nt, preferred_element_type=F32) + lax.dot_general(
            query, mem_lo, nt, preferred_element_type=F32
        )
        old_read = jnp.zeros((seqs, HEAD_SIZE), F32)
        for s in range(seqs):
            old_read = old_read + jnp.where(
                sub == s, read[:, s * HEAD_SIZE : (s + 1) * HEAD_SIZE], 0.0
            )
        numerator = keep * old_read + (write * key_query) * value_f
        floor_value = jnp.maximum(jnp.maximum(jnp.abs(denominator), jnp.exp(-new_max)), 1.0)
        gated = (jax.nn.sigmoid(outgate) * (numerator / floor_value)).astype(BF16)
        own_gated[layer] = gated

        gd = [
            send_dp(
                own_gated.at[layer],
                gated_slots.at[layer, dp],
                gd_send.at[layer, off],
                gd_recv.at[layer, off],
                off,
            )
            for off in range(1, n_dp)
        ]
        gated_slots[layer, dp] = gated
        new_normalizer[layer] = new_norm.reshape(seqs, 1, HEAD_SIZE)
        new_stabilizer[layer] = jnp.sum(
            jnp.where(diag_seq, jnp.broadcast_to(new_max, (seqs, seqs)), 0.0), axis=0, keepdims=True
        )
        out_copies[layer].wait()
        for copy in gd:
            copy.wait_recv()
        all_gated = jnp.concatenate(
            [gated_slots[layer, d].astype(F32) for d in range(n_dp)], axis=0
        ).astype(BF16)
        partial = jnp.dot(all_gated, w_out_v[layer], preferred_element_type=F32)

        for t in range(n_tp):
            send_o[layer, t] = partial[t * rows : (t + 1) * rows].astype(BF16)
        ro = [
            send_tp(
                send_o.at[layer, tp_peer(off)],
                recv_o.at[layer, off],
                ro_send.at[layer, off],
                ro_recv.at[layer, off],
                off,
            )
            for off in range(1, n_tp)
        ]

        key_wide = jnp.concatenate(
            [jnp.where(sub == s, key.astype(F32), 0.0).astype(BF16) for s in range(seqs)], axis=1
        )
        outer = lax.dot_general(value, key_wide, tn, preferred_element_type=F32)
        write_scaled = write * scale
        for s in range(seqs):
            new_mem_v[layer, s, 0] = (
                keep[s : s + 1] * mem_v[layer, s, 0]
                + write_scaled[s : s + 1] * outer[:, s * HEAD_SIZE : (s + 1) * HEAD_SIZE]
            )
        update = pltpu.make_async_copy(new_mem_v.at[layer], new_memory.at[layer], out_sem.at[layer])
        update.start()
        updates.append(update)

        summed = send_o[layer, tp].astype(F32)
        for off in range(1, n_tp):
            ro[off - 1].wait_recv()
            summed = summed + recv_o[layer, off].astype(F32)
        result = (own_x[layer].astype(F32) + summed).astype(BF16)
        if layer == 0:
            own_x[1] = result
            ag = gather_x(1)
        else:
            mixed[...] = result
    for copy in started:
        copy.wait_send()
    for copy in updates:
        copy.wait()


def body(
    n_tp,
    n_dp,
    tokens,
    norm_gain,
    w_query,
    w_key,
    w_value,
    w_outgate,
    w_gates,
    gate_bias,
    w_out,
    memory,
    normalizer,
    stabilizer,
):
    rows, width = tokens.shape
    seqs, heads_here = memory.shape[1:3]
    assert heads_here == 1
    gate_columns = w_gates.shape[2]
    hbm = pl.BlockSpec(memory_space=pl.ANY)
    vmem = pl.BlockSpec(memory_space=pltpu.VMEM)
    dma = pltpu.SemaphoreType.DMA
    moved = 2 * (5 * width * HEAD_SIZE * 2 + 2 * seqs * HEAD_SIZE * HEAD_SIZE * 4)
    mixed, new_memory, new_normalizer, new_stabilizer = pl.pallas_call(
        functools.partial(kernel, n_tp, n_dp),
        out_shape=(
            jax.ShapeDtypeStruct(tokens.shape, BF16),
            jax.ShapeDtypeStruct(memory.shape, F32),
            jax.ShapeDtypeStruct(normalizer.shape, F32),
            jax.ShapeDtypeStruct((2, heads_here, seqs), F32),
        ),
        in_specs=[hbm] * 12,
        out_specs=(vmem, hbm, vmem, vmem),
        scratch_shapes=[
            pltpu.VMEM((2, width), BF16),
            pltpu.VMEM((2, width, 4 * HEAD_SIZE), BF16),
            pltpu.VMEM((2, gate_columns, width), BF16),
            pltpu.VMEM((2, 1, 2), F32),
            pltpu.VMEM((2, HEAD_SIZE, width), BF16),
            pltpu.VMEM(memory.shape, F32),
            pltpu.VMEM(normalizer.shape, F32),
            pltpu.VMEM((2, 1, seqs), F32),
            pltpu.VMEM(memory.shape, F32),
            pltpu.VMEM((2, rows, width), BF16),
            pltpu.VMEM((2, n_tp, rows, width), BF16),
            pltpu.VMEM((2, n_dp, seqs, 4 * HEAD_SIZE), BF16),
            pltpu.VMEM((2, n_dp, seqs, 4 * HEAD_SIZE), BF16),
            pltpu.VMEM((2, n_dp, seqs, HEAD_SIZE), F32),
            pltpu.VMEM((2, n_dp, seqs, HEAD_SIZE), F32),
            pltpu.VMEM((2, seqs, HEAD_SIZE), BF16),
            pltpu.VMEM((2, n_dp, seqs, HEAD_SIZE), BF16),
            pltpu.VMEM((2, n_tp, rows, width), BF16),
            pltpu.VMEM((2, n_tp, rows, width), BF16),
            dma((6,)),
            dma((2, 5)),
            dma((2,)),
            dma((2,)),
            dma((2, n_tp)),
            dma((2, n_tp)),
            dma((2, n_dp)),
            dma((2, n_dp)),
            dma((2, n_dp)),
            dma((2, n_dp)),
            dma((2, n_dp)),
            dma((2, n_dp)),
            dma((2, n_tp)),
            dma((2, n_tp)),
        ],
        compiler_params=pltpu.CompilerParams(
            collective_id=0, has_side_effects=True, vmem_limit_bytes=60 * 1024 * 1024
        ),
        cost_estimate=pl.CostEstimate(
            flops=2 * 2 * n_tp * rows * width * 5 * HEAD_SIZE, bytes_accessed=moved, transcendentals=0
        ),
    )(
        tokens,
        norm_gain,
        w_query,
        w_key,
        w_value,
        w_outgate,
        jnp.swapaxes(w_gates, 1, 2),
        jnp.swapaxes(gate_bias, 1, 2),
        w_out,
        memory,
        normalizer,
        jnp.swapaxes(stabilizer, 1, 2),
    )
    return mixed, new_memory, new_normalizer, jnp.swapaxes(new_stabilizer, 1, 2)


def solution(mesh):
    placed = (
        P("tp", "dp"),
        P(None, "dp"),
        P(None, "dp", "tp"),
        P(None, "dp", "tp"),
        P(None, "dp", "tp"),
        P(None, "dp", "tp"),
        P(None, "dp", None),
        P(None, None, "tp"),
        P(None, "tp", "dp"),
        P(None, "dp", "tp", None, None),
        P(None, "dp", "tp", None),
        P(None, "dp", "tp"),
    )
    return jax.shard_map(
        functools.partial(body, mesh.shape["tp"], mesh.shape["dp"]),
        mesh=mesh,
        in_specs=placed,
        out_specs=(
            P("tp", "dp"),
            P(None, "dp", "tp", None, None),
            P(None, "dp", "tp", None),
            P(None, "dp", "tp"),
        ),
        check_vma=False,
    )
```

time: 270 us -> 42.3 us (0.16)
  waiting for transfers between devices: 188 us -> 0 us
  Pallas kernels: 0 us -> 36.6 us
  blocking collectives: 33.7 us -> 0 us
  other arithmetic: 16.8 us -> 0 us
  between operations: 15.2 us -> 0.66 us
  matrix products: 11.1 us -> 0 us
    unnamed x7 -> x0, waiting for transfers between devices: 133 us -> none
    psum x1 -> x0, waiting for transfers between devices: 55.4 us -> none  [body(): summed = lax.psum(partial_out, 'tp')]
    pallas_call x0 -> x1, Pallas kernels: none -> 36.6 us  [body(): pl.pallas_call(functools.partial(kernel, n_tp, n_dp), out_shape=(jax.Shap...]
    all_gather x3 -> x0, blocking collectives: 33.7 us -> none  [the longest x2 17.8 us: body(): lax.all_gather(gated, 'dp', axis=0, tiled=True)]
    dot_general x12 -> x0, matrix products: 11.1 us -> none  [the longest x2 2.53 us: body(): jnp.dot(scaled, w_outgate[layer_index], preferred_element_type=jnp.float32)]
    reduce_sum x6 -> x0, other arithmetic: 4.74 us -> none  [the longest x2 2.2 us: body(): square_part = jnp.sum(wide_rows * wide_rows, axis=1)]
    mul x7 -> x0, other arithmetic: 4.22 us -> none  [the longest x2 2.65 us: cell_update(): write_factor[:, :, None] * key_float]
    another operation x5 -> x0, other arithmetic: 3.75 us -> none  [the longest x3 2.11 us: body(): jnp.stack(normalizers)]
  transfers between devices with their start and end apart: 4 -> 0, of which waited for: 4 -> 0; matrix products, arithmetic and copies ran while one was open for 2% -> 0% of each run, Pallas kernels for 0% -> 0%
where the time goes in v1:
time: 42.3 us; the launch traced here: 42 us
  Pallas kernels  36.6 us (87%)
  local copies, waits for them, and re-layouts  4.82 us (11%)
  between operations  0.66 us (2%)
    pallas_call x1, Pallas kernels, body(): pl.pallas_call(functools.partial(kernel, n_tp, n_dp), out_shape=(jax.Shap...  36.6 us
    unnamed x10, local copies, waits for them, and re-layouts  4.82 us

profile of v1, /device:TPU:0, one launch (start us, length us, event | category | flops | bytes accessed | tf_op | source)
XLA Modules:
  0.0 42.0 jit_solution(6413779128216128231)
XLA Ops:
  0.6 36.6 %shard_map.147 = (bf16[4,1024]{1,0:T(4,128)(2,1)}, f32[2,8,1,128,128]{4,3,2,1,0:T(8,128)}, f32[2,8,1,128]{3,2,1,0:T(1,128)}, f32[2,1,8]{2,1,0:T(1,128)}) custom-call(bf16[4,1024]{1,0:T(4,128)(2,1)} %tokens.1, bf16[2,1024]{1,0:T(2,128)(2,1)} %norm_gain.1, bf16[2,1024,128]{2,1,0:T(8,128)(2,1)} %w_query.1, bf16[2,1024,128]{2,1,0:T(8,128)(2,1)} %w_key.1, ...), custom_call_target="tpu_custom_call" | custom-call | flops 83886080 | bytes 4718592 | tf_op jit(solution)/shard_map/pallas_call | solution.py:361
  37.2 0.0 copy-start.1
  37.2 0.7 %copy-done.1 = bf16[4,1024]{1,0:T(4,128)(2,1)S(1)} copy-done((bf16[4,1024]{1,0:T(4,128)(2,1)S(1)}, bf16[4,1024]{1,0:T(4,128)(2,1)}, u32[]{:S(2)}) %copy-start.1) | copy-done | bytes 8216
  37.9 0.6 %copy.23 = bf16[4,1024]{1,0:T(4,128)(2,1)} copy(bf16[4,1024]{1,0:T(4,128)(2,1)S(1)} %copy-done.1) | data formatting | bytes 16384
  38.5 0.0 copy-start
  38.5 2.3 %copy.24 = f32[2,8,1,128,128]{4,3,2,1,0:T(8,128)} copy(f32[2,8,1,128,128]{4,3,2,1,0:T(8,128)} %get-tuple-element.21) | data formatting | bytes 2097152
  40.8 0.0 copy-done
  40.8 0.0 copy-start.2
  40.8 0.6 %copy.25 = f32[2,8,1,128]{3,2,1,0:T(1,128)} copy(f32[2,8,1,128]{3,2,1,0:T(1,128)S(1)} %copy-done) | data formatting | bytes 16384
  41.4 0.1 copy-done.2
  41.5 0.6 %copy.26 = f32[2,8,1]{1,2,0:T(1,128)} copy(f32[2,8,1]{1,2,0:T(1,128)S(1)} %bitcast.11) | data formatting | bytes 128
Async XLA Ops:
  37.2 0.7 %copy-start.1 = (bf16[4,1024]{1,0:T(4,128)(2,1)S(1)}, bf16[4,1024]{1,0:T(4,128)(2,1)}, u32[]{:S(2)}) copy-start(bf16[4,1024]{1,0:T(4,128)(2,1)} %get-tuple-element.20) | copy-start | bytes 24580
  38.5 2.3 %copy-start = (f32[2,8,1,128]{3,2,1,0:T(1,128)S(1)}, f32[2,8,1,128]{3,2,1,0:T(1,128)}, u32[]{:S(2)}) copy-start(f32[2,8,1,128]{3,2,1,0:T(1,128)} %get-tuple-element.22) | copy-start | bytes 24580
  40.8 0.7 %copy-start.2 = (f32[2,1,8]{2,1,0:T(1,128)S(1)}, f32[2,1,8]{2,1,0:T(1,128)}, u32[]{:S(2)}) copy-start(f32[2,1,8]{2,1,0:T(1,128)} %get-tuple-element.11) | copy-start | bytes 196

commit v2 on v1

--- a/solution.py
+++ b/solution.py
@@ -41,7 +41,6 @@
     mem_v,
     norm_v,
     stab_v,
-    new_mem_v,
     own_x,
     x_slots,
     send_q,
@@ -55,7 +54,6 @@
     in_sem,
     w_sem,
     mem_sem,
-    out_sem,
     ag_send,
     ag_recv,
     rq_send,
@@ -76,18 +74,27 @@
     heads = w_gates_v.shape[1] // 2
     features = width * n_dp
 
-    def tp_peer(off):
-        return lax.rem(tp + off, n_tp)
-
-    def dp_peer(off):
-        return lax.rem(dp + off, n_dp)
+    def flip(index, mask):
+        for bit in range(mask.bit_length()):
+            if mask >> bit & 1:
+                index = index + (1 - 2 * (index // 2**bit % 2)) * 2**bit
+        return index
+
+    def tp_peer(mask):
+        return flip(tp, mask)
+
+    def dp_peer(mask):
+        return flip(dp, mask)
+
+    tp_masks = range(n_tp - 1, 0, -1)
+    dp_masks = range(n_dp - 1, 0, -1)
 
     barrier = pltpu.get_barrier_semaphore()
     tok_copy = pltpu.make_async_copy(tokens, own_x.at[0], in_sem.at[0])
     tok_copy.start()
-    for off in range(1, n_tp):
+    for off in tp_masks:
         pl.semaphore_signal(barrier, inc=1, device_id={"tp": tp_peer(off)}, device_id_type=MESH)
-    for off in range(1, n_dp):
+    for off in dp_masks:
         pl.semaphore_signal(barrier, inc=1, device_id={"dp": dp_peer(off)}, device_id_type=MESH)
 
     small = [
@@ -158,7 +165,7 @@
                 ag_recv.at[layer, off],
                 off,
             )
-            for off in range(1, n_tp)
+            for off in tp_masks
         ]
         x_slots[layer, tp] = own_x[layer]
         return copies
@@ -171,11 +178,13 @@
     scale = HEAD_SIZE ** (-0.5)
     nt = (((1,), (1,)), ((), ()))
     tn = (((0,), (0,)), ((), ()))
-    updates = []
 
     ag = gather_x(0)
     for copy in small:
         copy.wait()
+    for layer in range(2):
+        columns = w_gates_v[layer].astype(F32).T.astype(BF16)
+        w_in_v[layer, :, 4 * HEAD_SIZE : 4 * HEAD_SIZE + 2 * heads] = columns
     for layer in range(2):
         for copy in w_copies[layer]:
             copy.wait()
@@ -189,47 +198,45 @@
             copy.wait_recv()
         wide = jnp.concatenate([x_slots[layer, t].astype(F32) for t in range(n_tp)], axis=0)
         scaled = (wide * gain).astype(BF16)
-        terms = jnp.dot(scaled, w_in_v[layer], preferred_element_type=F32).astype(BF16)
-        for d in range(n_dp):
-            send_q[layer, d] = terms[d * seqs : (d + 1) * seqs]
-        rq = [
-            send_dp(
-                send_q.at[layer, dp_peer(off)],
-                recv_q.at[layer, off],
-                rq_send.at[layer, off],
-                rq_recv.at[layer, off],
-                off,
-            )
-            for off in range(1, n_dp)
-        ]
+        terms = jnp.dot(scaled, w_in_v[layer], preferred_element_type=F32)
         squares = jnp.sum(wide * wide, axis=1, keepdims=True)
-        gates = lax.dot_general(scaled, w_gates_v[layer], nt, preferred_element_type=F32)
-        column = lax.broadcasted_iota(jnp.int32, gates.shape, 1)
-        gate_in = jnp.sum(jnp.where(column == tp, gates, 0.0), axis=1, keepdims=True)
-        gate_forget = jnp.sum(jnp.where(column == heads + tp, gates, 0.0), axis=1, keepdims=True)
+        gates = terms[:, 4 * HEAD_SIZE :]
+        gate_in = jnp.sum(jnp.where(lane == tp, gates, 0.0), axis=1, keepdims=True)
+        gate_forget = jnp.sum(jnp.where(lane == heads + tp, gates, 0.0), axis=1, keepdims=True)
         packed = jnp.where(
             lane == 0, gate_in, jnp.where(lane == 1, gate_forget, jnp.where(lane == 2, squares, 0.0))
         )
         for d in range(n_dp):
+            send_q[layer, d] = terms[d * seqs : (d + 1) * seqs, : 4 * HEAD_SIZE].astype(BF16)
             send_g[layer, d] = packed[d * seqs : (d + 1) * seqs]
-        rg = [
-            send_dp(
-                send_g.at[layer, dp_peer(off)],
-                recv_g.at[layer, off],
-                rg_send.at[layer, off],
-                rg_recv.at[layer, off],
-                off,
-            )
-            for off in range(1, n_dp)
-        ]
+        rq, rg = [], []
+        for off in dp_masks:
+            rg.append(
+                send_dp(
+                    send_g.at[layer, dp_peer(off)],
+                    recv_g.at[layer, off],
+                    rg_send.at[layer, off],
+                    rg_recv.at[layer, off],
+                    off,
+                )
+            )
+            rq.append(
+                send_dp(
+                    send_q.at[layer, dp_peer(off)],
+                    recv_q.at[layer, off],
+                    rq_send.at[layer, off],
+                    rq_recv.at[layer, off],
+                    off,
+                )
+            )
 
         sums = send_q[layer, dp].astype(F32)
         small_sums = send_g[layer, dp]
-        for off in range(1, n_dp):
-            rq[off - 1].wait_recv()
+        for off in dp_masks:
+            rq[n_dp - 1 - off].wait_recv()
             sums = sums + recv_q[layer, off].astype(F32)
-        for off in range(1, n_dp):
-            rg[off - 1].wait_recv()
+        for off in dp_masks:
+            rg[n_dp - 1 - off].wait_recv()
             small_sums = small_sums + recv_g[layer, off]
         inv = lax.rsqrt(small_sums[:, 2:3] / features + EPSILON)
         held = (sums * inv).astype(BF16)
@@ -276,7 +283,7 @@
                 gd_recv.at[layer, off],
                 off,
             )
-            for off in range(1, n_dp)
+            for off in dp_masks
         ]
         gated_slots[layer, dp] = gated
         new_normalizer[layer] = new_norm.reshape(seqs, 1, HEAD_SIZE)
@@ -301,7 +308,7 @@
                 ro_recv.at[layer, off],
                 off,
             )
-            for off in range(1, n_tp)
+            for off in tp_masks
         ]
 
         key_wide = jnp.concatenate(
@@ -310,17 +317,14 @@
         outer = lax.dot_general(value, key_wide, tn, preferred_element_type=F32)
         write_scaled = write * scale
         for s in range(seqs):
-            new_mem_v[layer, s, 0] = (
+            new_memory[layer, s, 0] = (
                 keep[s : s + 1] * mem_v[layer, s, 0]
                 + write_scaled[s : s + 1] * outer[:, s * HEAD_SIZE : (s + 1) * HEAD_SIZE]
             )
-        update = pltpu.make_async_copy(new_mem_v.at[layer], new_memory.at[layer], out_sem.at[layer])
-        update.start()
-        updates.append(update)
 
         summed = send_o[layer, tp].astype(F32)
-        for off in range(1, n_tp):
-            ro[off - 1].wait_recv()
+        for off in tp_masks:
+            ro[n_tp - 1 - off].wait_recv()
             summed = summed + recv_o[layer, off].astype(F32)
         result = (own_x[layer].astype(F32) + summed).astype(BF16)
         if layer == 0:
@@ -330,7 +334,17 @@
             mixed[...] = result
     for copy in started:
         copy.wait_send()
-    for copy in updates:
+
+
+def write_out(*refs):
+    sources, targets, sem = refs[:4], refs[4:8], refs[8]
+    copies = [
+        pltpu.make_async_copy(source, target, sem.at[i])
+        for i, (source, target) in enumerate(zip(sources, targets))
+    ]
+    for copy in copies:
+        copy.start()
+    for copy in copies:
         copy.wait()
 
 
@@ -358,26 +372,25 @@
     vmem = pl.BlockSpec(memory_space=pltpu.VMEM)
     dma = pltpu.SemaphoreType.DMA
     moved = 2 * (5 * width * HEAD_SIZE * 2 + 2 * seqs * HEAD_SIZE * HEAD_SIZE * 4)
-    mixed, new_memory, new_normalizer, new_stabilizer = pl.pallas_call(
+    results = pl.pallas_call(
         functools.partial(kernel, n_tp, n_dp),
         out_shape=(
-            jax.ShapeDtypeStruct(tokens.shape, BF16),
-            jax.ShapeDtypeStruct(memory.shape, F32),
-            jax.ShapeDtypeStruct(normalizer.shape, F32),
-            jax.ShapeDtypeStruct((2, heads_here, seqs), F32),
+            pltpu.VMEM(tokens.shape, BF16),
+            pltpu.VMEM(memory.shape, F32),
+            pltpu.VMEM(normalizer.shape, F32),
+            pltpu.VMEM((2, heads_here, seqs), F32),
         ),
         in_specs=[hbm] * 12,
-        out_specs=(vmem, hbm, vmem, vmem),
+        out_specs=(vmem,) * 4,
         scratch_shapes=[
             pltpu.VMEM((2, width), BF16),
-            pltpu.VMEM((2, width, 4 * HEAD_SIZE), BF16),
+            pltpu.VMEM((2, width, 5 * HEAD_SIZE), BF16),
             pltpu.VMEM((2, gate_columns, width), BF16),
             pltpu.VMEM((2, 1, 2), F32),
             pltpu.VMEM((2, HEAD_SIZE, width), BF16),
             pltpu.VMEM(memory.shape, F32),
             pltpu.VMEM(normalizer.shape, F32),
             pltpu.VMEM((2, 1, seqs), F32),
-            pltpu.VMEM(memory.shape, F32),
             pltpu.VMEM((2, rows, width), BF16),
             pltpu.VMEM((2, n_tp, rows, width), BF16),
             pltpu.VMEM((2, n_dp, seqs, 4 * HEAD_SIZE), BF16),
@@ -390,7 +403,6 @@
             pltpu.VMEM((2, n_tp, rows, width), BF16),
             dma((6,)),
             dma((2, 5)),
-            dma((2,)),
             dma((2,)),
             dma((2, n_tp)),
             dma((2, n_tp)),
@@ -423,6 +435,13 @@
         normalizer,
         jnp.swapaxes(stabilizer, 1, 2),
     )
+    mixed, new_memory, new_normalizer, new_stabilizer = pl.pallas_call(
+        write_out,
+        out_shape=[jax.ShapeDtypeStruct(r.shape, r.dtype) for r in results],
+        in_specs=[vmem] * 4,
+        out_specs=[hbm] * 4,
+        scratch_shapes=[dma((4,))],
+    )(*(pltpu.with_memory_space_constraint(r, pltpu.VMEM) for r in results))
     return mixed, new_memory, new_normalizer, jnp.swapaxes(new_stabilizer, 1, 2)
 
 

time: 42.3 us -> 37.6 us (0.89)
  local copies, waits for them, and re-layouts: 4.82 us -> 0 us
    unnamed x10 -> x0, local copies, waits for them, and re-layouts: 4.82 us -> none
    pallas_call x1 -> x2, Pallas kernels: 36.6 us -> 36.7 us  [the longest x1 35.7 us: body(): pl.pallas_call(functools.partial(kernel, n_tp, n_dp), out_shape=(pltpu.VM...]
where the time goes in v2:
time: 37.6 us; the launch traced here: 37.4 us
  Pallas kernels  36.7 us (98%)
  between operations  0.64 us (2%)
    pallas_call x1, Pallas kernels, body(): pl.pallas_call(functools.partial(kernel, n_tp, n_dp), out_shape=(pltpu.VM...  35.7 us
    pallas_call x1, Pallas kernels, body(): pl.pallas_call(write_out, out_shape=[jax.ShapeDtypeStruct(r.shape, r.dtyp...  1.02 us

profile of v2, /device:TPU:0, one launch (start us, length us, event | category | flops | bytes accessed | tf_op | source)
XLA Modules:
  0.0 37.4 jit_solution(17549183450574356259)
XLA Ops:
  0.6 35.7 %shard_map.147 = (bf16[4,1024]{1,0:T(4,128)(2,1)S(1)}, f32[2,8,1,128,128]{4,3,2,1,0:T(8,128)S(1)}, f32[2,8,1,128]{3,2,1,0:T(1,128)S(1)}, f32[2,1,8]{2,1,0:T(1,128)S(1)}) custom-call(bf16[4,1024]{1,0:T(4,128)(2,1)} %tokens.1, bf16[2,1024]{1,0:T(2,128)(2,1)} %norm_gain.1, bf16[2,1024,128]{2,1,0:T(8,128)(2,1)} %w_query.1, bf16[2,1024,128]{2,1,0:T(8,128)(2,1)} %w_key.1, ...), custom_call_target="tpu_custom_call" | custom-call | flops 83886080 | bytes 4718592 | tf_op jit(solution)/shard_map/pallas_call | solution.py:375
  36.3 1.0 %shard_map.148 = (bf16[4,1024]{1,0:T(4,128)(2,1)}, f32[2,8,1,128,128]{4,3,2,1,0:T(8,128)}, f32[2,8,1,128]{3,2,1,0:T(1,128)}, f32[2,1,8]{2,1,0:T(1,128)}) custom-call(bf16[4,1024]{1,0:T(4,128)(2,1)S(1)} %get-tuple-element.12.refs_0_, f32[2,8,1,128,128]{4,3,2,1,0:T(8,128)S(1)} %get-tuple-element.13.refs_1_, f32[2,8,1,128]{3,2,1,0:T(1,128)S(1)} %get-tuple-element.14.refs_2_, ...), custom_call_target="tpu_custom_call" | custom-call | tf_op jit(solution)/shard_map/pallas_call | solution.py:438

commit v3 on v2

--- a/solution.py
+++ b/solution.py
@@ -51,6 +51,12 @@
     gated_slots,
     send_o,
     recv_o,
+    send_p,
+    recv_p,
+    own_pair,
+    recv_z,
+    own_half,
+    halves,
     in_sem,
     w_sem,
     mem_sem,
@@ -64,6 +70,10 @@
     gd_recv,
     ro_send,
     ro_recv,
+    pair_send,
+    pair_recv,
+    z_send,
+    z_recv,
 ):
     tp = lax.axis_index("tp")
     dp = lax.axis_index("dp")
@@ -86,6 +96,9 @@
     def dp_peer(mask):
         return flip(dp, mask)
 
+    core = lax.rem(tp, 2)
+    half = width // 2
+    chip_masks = range(n_tp - 2, 0, -2)
     tp_masks = range(n_tp - 1, 0, -1)
     dp_masks = range(n_dp - 1, 0, -1)
 
@@ -196,7 +209,10 @@
 
         for copy in ag:
             copy.wait_recv()
-        wide = jnp.concatenate([x_slots[layer, t].astype(F32) for t in range(n_tp)], axis=0)
+        if layer == 0:
+            wide = jnp.concatenate([x_slots[0, t].astype(F32) for t in range(n_tp)], axis=0)
+        else:
+            wide = jnp.concatenate([halves[0], halves[1]], axis=1).astype(F32)
         scaled = (wide * gain).astype(BF16)
         terms = jnp.dot(scaled, w_in_v[layer], preferred_element_type=F32)
         squares = jnp.sum(wide * wide, axis=1, keepdims=True)
@@ -298,40 +314,63 @@
         ).astype(BF16)
         partial = jnp.dot(all_gated, w_out_v[layer], preferred_element_type=F32)
 
-        for t in range(n_tp):
-            send_o[layer, t] = partial[t * rows : (t + 1) * rows].astype(BF16)
-        ro = [
-            send_tp(
-                send_o.at[layer, tp_peer(off)],
-                recv_o.at[layer, off],
-                ro_send.at[layer, off],
-                ro_recv.at[layer, off],
-                off,
+        def update_states():
+            key_wide = jnp.concatenate(
+                [jnp.where(sub == s, key.astype(F32), 0.0).astype(BF16) for s in range(seqs)], axis=1
             )
-            for off in tp_masks
-        ]
-
-        key_wide = jnp.concatenate(
-            [jnp.where(sub == s, key.astype(F32), 0.0).astype(BF16) for s in range(seqs)], axis=1
-        )
-        outer = lax.dot_general(value, key_wide, tn, preferred_element_type=F32)
-        write_scaled = write * scale
-        for s in range(seqs):
-            new_memory[layer, s, 0] = (
-                keep[s : s + 1] * mem_v[layer, s, 0]
-                + write_scaled[s : s + 1] * outer[:, s * HEAD_SIZE : (s + 1) * HEAD_SIZE]
-            )
-
-        summed = send_o[layer, tp].astype(F32)
-        for off in tp_masks:
-            ro[n_tp - 1 - off].wait_recv()
-            summed = summed + recv_o[layer, off].astype(F32)
-        result = (own_x[layer].astype(F32) + summed).astype(BF16)
+            outer = lax.dot_general(value, key_wide, tn, preferred_element_type=F32)
+            write_scaled = write * scale
+            for s in range(seqs):
+                new_memory[layer, s, 0] = (
+                    keep[s : s + 1] * mem_v[layer, s, 0]
+                    + write_scaled[s : s + 1] * outer[:, s * HEAD_SIZE : (s + 1) * HEAD_SIZE]
+                )
+
         if layer == 0:
-            own_x[1] = result
-            ag = gather_x(1)
+            first, second = partial[:, :half], partial[:, half:]
+            send_p[0] = first.astype(BF16)
+            send_p[1] = second.astype(BF16)
+            swap = send_tp(send_p.at[1 - core], recv_p, pair_send.at[0], pair_recv.at[0], 1)
+            own_part = jnp.where(core == 0, first, second)
+            swap.wait_recv()
+            pair = (own_part + recv_p[...].astype(F32)).astype(BF16)
+            own_pair[...] = pair
+            copies = [
+                send_tp(
+                    own_pair, recv_z.at[mask // 2], z_send.at[mask // 2], z_recv.at[mask // 2], mask
+                )
+                for mask in chip_masks
+            ]
+            update_states()
+            summed = jnp.where(core == 0, wide[:, :half], wide[:, half:]) + pair.astype(F32)
+            for mask, copy in zip(chip_masks, copies):
+                copy.wait_recv()
+                summed = summed + recv_z[mask // 2].astype(F32)
+            result = summed.astype(BF16)
+            own_half[...] = result
+            ag = [send_tp(own_half, halves.at[core], pair_send.at[1], pair_recv.at[1], 1)]
+            halves[core] = result
         else:
-            mixed[...] = result
+            for t in range(n_tp):
+                send_o[layer, t] = partial[t * rows : (t + 1) * rows].astype(BF16)
+            ro = [
+                send_tp(
+                    send_o.at[layer, tp_peer(off)],
+                    recv_o.at[layer, off],
+                    ro_send.at[layer, off],
+                    ro_recv.at[layer, off],
+                    off,
+                )
+                for off in tp_masks
+            ]
+            update_states()
+            summed = send_o[layer, tp].astype(F32)
+            for t in range(n_tp):
+                summed = summed + jnp.where(tp == t, wide[t * rows : (t + 1) * rows], 0.0)
+            for copy, off in zip(ro, tp_masks):
+                copy.wait_recv()
+                summed = summed + recv_o[layer, off].astype(F32)
+            mixed[...] = summed.astype(BF16)
     for copy in started:
         copy.wait_send()
 
@@ -401,6 +440,12 @@
             pltpu.VMEM((2, n_dp, seqs, HEAD_SIZE), BF16),
             pltpu.VMEM((2, n_tp, rows, width), BF16),
             pltpu.VMEM((2, n_tp, rows, width), BF16),
+            pltpu.VMEM((2, n_tp * rows, width // 2), BF16),
+            pltpu.VMEM((n_tp * rows, width // 2), BF16),
+            pltpu.VMEM((n_tp * rows, width // 2), BF16),
+            pltpu.VMEM((n_tp // 2, n_tp * rows, width // 2), BF16),
+            pltpu.VMEM((n_tp * rows, width // 2), BF16),
+            pltpu.VMEM((2, n_tp * rows, width // 2), BF16),
             dma((6,)),
             dma((2, 5)),
             dma((2,)),
@@ -414,6 +459,10 @@
             dma((2, n_dp)),
             dma((2, n_tp)),
             dma((2, n_tp)),
+            dma((2,)),
+            dma((2,)),
+            dma((n_tp // 2,)),
+            dma((n_tp // 2,)),
         ],
         compiler_params=pltpu.CompilerParams(
             collective_id=0, has_side_effects=True, vmem_limit_bytes=60 * 1024 * 1024

time: 37.6 us -> 36.7 us (0.976)
  Pallas kernels: 36.7 us -> 35.9 us
    pallas_call x1, Pallas kernels: 35.7 us -> 34.9 us  [body(): pl.pallas_call(functools.partial(kernel, n_tp, n_dp), out_shape=(pltpu.VM...]
where the time goes in v3:
time: 36.7 us; the launch traced here: 36.5 us
  Pallas kernels  35.9 us (98%)
  between operations  0.64 us (2%)
    pallas_call x1, Pallas kernels, body(): pl.pallas_call(functools.partial(kernel, n_tp, n_dp), out_shape=(pltpu.VM...  34.9 us
    pallas_call x1, Pallas kernels, body(): pl.pallas_call(write_out, out_shape=[jax.ShapeDtypeStruct(r.shape, r.dtyp...  1.02 us

profile of v3, /device:TPU:0, one launch (start us, length us, event | category | flops | bytes accessed | tf_op | source)
XLA Modules:
  0.0 36.5 jit_solution(4270812849211544665)
XLA Ops:
  0.6 34.9 %shard_map.147 = (bf16[4,1024]{1,0:T(4,128)(2,1)S(1)}, f32[2,8,1,128,128]{4,3,2,1,0:T(8,128)S(1)}, f32[2,8,1,128]{3,2,1,0:T(1,128)S(1)}, f32[2,1,8]{2,1,0:T(1,128)S(1)}) custom-call(bf16[4,1024]{1,0:T(4,128)(2,1)} %tokens.1, bf16[2,1024]{1,0:T(2,128)(2,1)} %norm_gain.1, bf16[2,1024,128]{2,1,0:T(8,128)(2,1)} %w_query.1, bf16[2,1024,128]{2,1,0:T(8,128)(2,1)} %w_key.1, ...), custom_call_target="tpu_custom_call" | custom-call | flops 83886080 | bytes 4718592 | tf_op jit(solution)/shard_map/pallas_call | solution.py:414
  35.5 1.0 %shard_map.148 = (bf16[4,1024]{1,0:T(4,128)(2,1)}, f32[2,8,1,128,128]{4,3,2,1,0:T(8,128)}, f32[2,8,1,128]{3,2,1,0:T(1,128)}, f32[2,1,8]{2,1,0:T(1,128)}) custom-call(bf16[4,1024]{1,0:T(4,128)(2,1)S(1)} %get-tuple-element.12.refs_0_, f32[2,8,1,128,128]{4,3,2,1,0:T(8,128)S(1)} %get-tuple-element.13.refs_1_, f32[2,8,1,128]{3,2,1,0:T(1,128)S(1)} %get-tuple-element.14.refs_2_, ...), custom_call_target="tpu_custom_call" | custom-call | tf_op jit(solution)/shard_map/pallas_call | solution.py:487
